TPU v7x, 32 devices: a whole 2x2x4 slice. The times are simulated.
32 devices in a mesh: fs: 16 (over z, y, x), tp: 2 (over core).
Axes of the slice: x: 2, y: 2, z: 4, core: 2. Of those that a mesh axis runs over, the one named last changes fastest.
Arguments:
- tokens: bfloat16 [12288, 2048], P('fs'), may hold values from -6 to 6
- norm_gain: float32 [2048], replicated, may hold values from 0.1 to 1.9
- gate_weight: float32 [2048, 5120], P('fs', 'tp'), may hold values from -0.125 to 0.125
- value_weight: float32 [2048, 5120], P('fs', 'tp'), may hold values from -0.125 to 0.125
- gate_scale: float32 [5120], P('tp'), may hold values from 0.3 to 3
- value_scale: float32 [5120], P('tp'), may hold values from 0.3 to 3
- gate_kernel: float32 [3, 5120], P(None, 'tp'), may hold values from -3.5 to 3.5
- value_kernel: float32 [3, 5120], P(None, 'tp'), may hold values from -3.5 to 3.5
- gate_bias: float32 [5120], P('tp'), may hold values from -3 to 3
- value_bias: float32 [5120], P('tp'), may hold values from -3 to 3
- down_weight: float32 [5120, 2048], P('tp', 'fs'), may hold values from -0.078125 to 0.078125
- down_scale: float32 [2048], P('tp'), may hold values from 0.3 to 3
Outputs:
- mixed: bfloat16 [12288, 2048], P('fs', 'tp')
All inputs are finite; a program needn't handle non-finite values.
Results may differ from a plain program's by a relative error of at most 0.014.
Values may be sent and summed in bfloat16 or wider, within the bound.
A program may use at most 128 MiB of HBM per device.

v0:
```python
import jax
import jax.numpy as jnp
from jax import lax
from jax.sharding import PartitionSpec as P

epsilon = 1e-06


def from_behind(value, axis, steps):
    count = lax.axis_size(axis)
    leading, last = (max(0, -steps), min(count, count - steps))
    return lax.ppermute(value, axis, [(source, source + steps) for source in range(leading, last)])


def normalize(tokens, norm_gain):
    values = tokens.astype(jnp.float32)
    scaled = values * lax.rsqrt(jnp.mean(values * values, axis=1, keepdims=True) + epsilon)
    return (scaled * norm_gain[None, :]).astype(jnp.bfloat16)


def causal_mix(current, previous, kernel, tap_bias):
    row_count = current.shape[0]
    joined = jnp.concatenate([previous, current], axis=0).astype(jnp.float32)
    summed_taps = tap_bias[None, :] + kernel[2][None, :] * joined[2:]
    for back_by in (1, 2):
        summed_taps = (
            summed_taps
            + kernel[2 - back_by][None, :] * joined[2 - back_by : 2 - back_by + row_count]
        )
    return summed_taps


def body(
    tokens,
    norm_gain,
    gate_weight,
    value_weight,
    gate_scale,
    value_scale,
    gate_kernel,
    value_kernel,
    gate_bias,
    value_bias,
    down_weight,
    down_scale,
):
    normed = normalize(tokens, norm_gain)
    gate_low = gate_weight.astype(jnp.bfloat16)
    value_low = value_weight.astype(jnp.bfloat16)
    down_low = down_weight.astype(jnp.bfloat16)
    row_count = normed.shape[0]
    gate_full, value_full, down_full = (
        lax.all_gather(gate_low, "fs", axis=0, tiled=True),
        lax.all_gather(value_low, "fs", axis=0, tiled=True),
        lax.all_gather(down_low, "fs", axis=1, tiled=True),
    )
    gate_raw = jnp.dot(normed, gate_full, preferred_element_type=jnp.float32)
    value_raw = jnp.dot(normed, value_full, preferred_element_type=jnp.float32)
    gate_pre = (gate_raw * gate_scale[None, :]).astype(jnp.bfloat16)
    value_pre = (value_raw * value_scale[None, :]).astype(jnp.bfloat16)
    previous_gate, previous_value = from_behind(
        (gate_pre[row_count - 2 :], value_pre[row_count - 2 :]), "fs", 1
    )
    gate_conv = causal_mix(gate_pre, previous_gate, gate_kernel, gate_bias)
    value_conv = causal_mix(value_pre, previous_value, value_kernel, value_bias)
    hidden = (jax.nn.gelu(gate_conv, approximate=True) * value_conv).astype(jnp.bfloat16)
    partial_terms = jnp.dot(hidden, down_full, preferred_element_type=jnp.float32)
    summed = lax.psum_scatter(
        partial_terms.astype(jnp.bfloat16), "tp", scatter_dimension=1, tiled=True
    ).astype(jnp.float32)
    return (summed * down_scale[None, :]).astype(jnp.bfloat16)


def solution(mesh):
    return jax.shard_map(
        body,
        mesh=mesh,
        in_specs=(
            P("fs", None),
            P(),
            P("fs", "tp"),
            P("fs", "tp"),
            P("tp"),
            P("tp"),
            P(None, "tp"),
            P(None, "tp"),
            P("tp"),
            P("tp"),
            P("tp", "fs"),
            P("tp"),
        ),
        out_specs=P("fs", "tp"),
        check_vma=False,
    )
```

profile of v0, /device:TPU:1, one launch (start us, length us, event | category | flops | bytes accessed | tf_op | source)
XLA Modules:
  0.0 492.5 jit_solution(2098866098435934052)
XLA Ops:
  6.5 0.0 copy-start.4
  6.5 0.0 copy-start.3
  6.5 0.0 copy-start.2
  6.5 0.0 copy-start.10
  6.5 0.0 copy-start.6
  6.5 0.0 all-gather.4.cloned.1.call-start
  6.6 2.4 convert_element_type.41
  9.0 0.0 all-gather.4.cloned.1.call-update
  9.0 0.0 all-gather.6.cloned.1.call-start
  9.1 2.2 convert_element_type.44
  11.3 0.0 all-gather.6.cloned.1.call-update
  11.3 0.0 all-gather.8.cloned.1.call-start
  11.4 2.2 convert_element_type.48
  13.6 0.0 all-gather.8.cloned.1.call-update
  13.6 0.0 reduce-scatter.2.cloned.1.call-start
  13.7 0.0 copy-done.4
  13.7 0.0 copy-done.3
  13.7 0.2 slice_reduce_fusion.2
  13.9 0.0 copy-done.2
  13.9 0.7 fusion.15
  14.6 0.0 copy-start.7
  14.6 127.9 %all-gather.4.cloned.1.call-done = bf16[2048,2560]{1,0:T(8,128)(2,1)} async-done(((bf16[128,2560]{1,0:T(8,128)(2,1)}), bf16[2048,2560]{1,0:T(8,128)(2,1)}) %all-gather.4.cloned.1.call-update) | async-done | bytes 10485776 | tf_op jit(solution)/shard_map/all_gather | solution.py:53
  142.5 0.0 copy-done.10
  142.5 0.0 copy-done.6
  142.5 11.1 %multiply_convert_fusion.1 = bf16[768,2560]{1,0:T(8,128)(2,1)S(1)} fusion(bf16[2048,2560]{1,0:T(8,128)(2,1)} %all-gather.4.cloned.1.call-done, f32[2560]{0:T(1024)S(1)} %copy-done.6, bf16[768,2048]{1,0:T(8,128)(2,1)S(1)} %copy-done.2, f32[2048]{0:T(1024)S(1)} %copy-done.10, f32[768]{0:T(1024)S(1)} %add_rsqrt_fusion), kind=kOutput, calls=%fused_computation.23 | convolution fusion | flops 8063287296 | bytes 17585152 | tf_op jit(solution)/shard_map/dot_general | solution.py:57
  153.6 0.0 copy-start
  153.6 1.9 copy-done
  155.5 3.1 collective-permute-start
  158.6 116.5 %all-gather.6.cloned.1.call-done = bf16[2048,2560]{1,0:T(8,128)(2,1)} async-done(((bf16[128,2560]{1,0:T(8,128)(2,1)}), bf16[2048,2560]{1,0:T(8,128)(2,1)}) %all-gather.6.cloned.1.call-update) | async-done | bytes 10485776 | tf_op jit(solution)/shard_map/all_gather | solution.py:54
  275.1 0.0 copy-done.7
  275.1 0.0 copy-start.1
  275.1 11.2 %multiply_convert_fusion = bf16[768,2560]{1,0:T(8,128)(2,1)S(1)} fusion(bf16[2048,2560]{1,0:T(8,128)(2,1)} %all-gather.6.cloned.1.call-done, f32[2560]{0:T(1024)S(1)} %copy-done.7, bf16[768,2048]{1,0:T(8,128)(2,1)S(1)} %copy-done.2, f32[2048]{0:T(1024)S(1)} %copy-done.10, f32[768]{0:T(1024)S(1)} %add_rsqrt_fusion), kind=kOutput, calls=%fused_computation.22 | convolution fusion | flops 8063287296 | bytes 17585152 | tf_op jit(solution)/shard_map/dot_general | solution.py:58
  286.3 3.2 collective-permute-start.1
  289.6 0.0 collective-permute-done
  289.6 0.0 copy-done.1
  289.6 4.4 maximum_convert_fusion
  294.0 0.0 copy-start.8
  294.0 0.0 copy-start.9
  294.0 0.0 collective-permute-done.1
  294.0 4.3 maximum_convert_fusion.1
  298.3 146.7 %all-gather.8.cloned.1.call-done = bf16[2560,2048]{1,0:T(8,128)(2,1)} async-done(((bf16[2560,128]{1,0:T(8,128)(2,1)}), bf16[2560,2048]{1,0:T(8,128)(2,1)}) %all-gather.8.cloned.1.call-update) | async-done | bytes 10485776 | tf_op jit(solution)/shard_map/all_gather | solution.py:55
  445.0 0.0 copy-done.8
  445.1 0.0 copy-done.9
  445.1 27.4 %fusion.20 = bf16[768,2048]{1,0:T(8,128)(2,1)} fusion(bf16[2560,2048]{1,0:T(8,128)(2,1)} %all-gather.8.cloned.1.call-done, f32[770,2560]{1,0:T(8,128)} %maximum_convert_fusion.1, f32[770,2560]{1,0:T(8,128)} %maximum_convert_fusion, f32[2560]{0:T(1024)S(1)} %get-tuple-element.9, f32[2560]{0:T(1024)S(1)} %get-tuple-element.10, ...), kind=kOutput, calls=%fused_computation.32 | convolution fusion | flops 8097890304 | bytes 60899328 | tf_op jit(solution)/shard_map/dot_general | solution.py:67
  472.5 0.0 reduce-scatter.2.cloned.1.call-update
  472.5 10.5 %reduce-scatter.2.cloned.1.call-done = bf16[768,1024]{1,0:T(8,128)(2,1)} async-done(((bf16[768,2048]{1,0:T(8,128)(2,1)}), bf16[768,1024]{1,0:T(8,128)(2,1)}) %reduce-scatter.2.cloned.1.call-update) | async-done | bytes 1572880 | tf_op jit(solution)/shard_map/reduce_scatter | solution.py:68
  483.0 0.0 copy-done.5
  483.0 3.0 multiply_convert_fusion.2
  (4 shorter events, 0.0 us)
Async XLA Ops:
  6.5 7.1 %copy-start.4 = (f32[3,2560]{1,0:T(4,128)S(1)}, f32[3,2560]{1,0:T(4,128)}, u32[]{:S(2)}) copy-start(f32[3,2560]{1,0:T(4,128)} %param.18) | copy-start | bytes 92164
  6.5 7.1 %copy-start.3 = (f32[3,2560]{1,0:T(4,128)S(1)}, f32[3,2560]{1,0:T(4,128)}, u32[]{:S(2)}) copy-start(f32[3,2560]{1,0:T(4,128)} %param.19) | copy-start | bytes 92164
  6.5 7.3 %copy-start.2 = (bf16[768,2048]{1,0:T(8,128)(2,1)S(1)}, bf16[768,2048]{1,0:T(8,128)(2,1)}, u32[]{:S(2)}) copy-start(bf16[768,2048]{1,0:T(8,128)(2,1)} %param.12) | copy-start | bytes 9437188
  6.5 135.9 %copy-start.10 = (f32[2048]{0:T(1024)S(1)}, f32[2048]{0:T(1024)}, u32[]{:S(2)}) copy-start(f32[2048]{0:T(1024)} %param.13) | copy-start | bytes 24580
  6.5 135.9 %copy-start.6 = (f32[2560]{0:T(1024)S(1)}, f32[2560]{0:T(1024)}, u32[]{:S(2)}) copy-start(f32[2560]{0:T(1024)} %param.16) | copy-start | bytes 30724
  6.5 135.9 %all-gather.4.cloned.1.call-start = ((), (), s32[]{:S(2)}) async-start(), calls=%async_computation.1 | async-start | bytes 11141120 | tf_op jit(solution)/shard_map/all_gather | solution.py:53
  9.0 266.1 %all-gather.6.cloned.1.call-start = ((), (), s32[]{:S(2)}) async-start(), calls=%async_computation.2 | async-start | bytes 11141120 | tf_op jit(solution)/shard_map/all_gather | solution.py:54
  11.3 433.7 %all-gather.8.cloned.1.call-start = ((), (), s32[]{:S(2)}) async-start(), calls=%async_computation.3 | async-start | bytes 11141120 | tf_op jit(solution)/shard_map/all_gather | solution.py:55
  13.6 469.4 %reduce-scatter.2.cloned.1.call-start = ((), (), s32[]{:S(2)}) async-start(), calls=%async_computation.4 | async-start | bytes 4718592 | tf_op jit(solution)/shard_map/reduce_scatter | solution.py:68
  14.6 260.5 %copy-start.7 = (f32[2560]{0:T(1024)S(1)}, f32[2560]{0:T(1024)}, u32[]{:S(2)}) copy-start(f32[2560]{0:T(1024)} %param.17) | copy-start | bytes 30724
  153.6 1.9 copy-start
  155.5 134.1 %collective-permute-start = (bf16[2,2560]{1,0:T(2,128)(2,1)S(1)}, bf16[2,2560]{1,0:T(2,128)(2,1)S(1)}, u32[]{:S(2)}, u32[]{:S(2)}) collective-permute-start(bf16[2,2560]{1,0:T(2,128)(2,1)S(1)} %slice.56), channel_id=1, source_target_pairs={{0,2},{2,4},{4,6},{6,8},{8,10},{10,12},{12,14},{14,16},{16,18},{18... | collective-permute-start | bytes 30728 | tf_op jit(solution)/shard_map/ppermute | solution.py:12
  275.1 14.5 %copy-start.1 = (bf16[768,2560]{1,0:T(8,128)(2,1)S(1)}, bf16[768,2560]{1,0:T(8,128)(2,1)}, u32[]{:S(2)}) copy-start(bf16[768,2560]{1,0:T(8,128)(2,1)} %copy-done) | copy-start | bytes 11796484
  286.3 7.6 %collective-permute-start.1 = (bf16[2,2560]{1,0:T(2,128)(2,1)S(1)}, bf16[2,2560]{1,0:T(2,128)(2,1)S(1)}, u32[]{:S(2)}, u32[]{:S(2)}) collective-permute-start(bf16[2,2560]{1,0:T(2,128)(2,1)S(1)} %slice.60), channel_id=1, source_target_pairs={{0,2},{2,4},{4,6},{6,8},{8,10},{10,12},{12,14},{14,16},{16,18},{18... | collective-permute-start | bytes 30728 | tf_op jit(solution)/shard_map/ppermute | solution.py:12
  294.0 151.1 %copy-start.8 = (f32[2560]{0:T(1024)S(1)}, f32[2560]{0:T(1024)}, u32[]{:S(2)}) copy-start(f32[2560]{0:T(1024)} %param.21) | copy-start | bytes 30724
  294.0 151.1 %copy-start.9 = (f32[2560]{0:T(1024)S(1)}, f32[2560]{0:T(1024)}, u32[]{:S(2)}) copy-start(f32[2560]{0:T(1024)} %param.20) | copy-start | bytes 30724
  445.1 38.0 %copy-start.5 = (f32[1024]{0:T(1024)S(1)}, f32[1024]{0:T(1024)}, u32[]{:S(2)}) copy-start(f32[1024]{0:T(1024)} %param.23) | copy-start | bytes 12292
Sparse Core Ops, SparseCore 0:
  10.0 132.3 all-gather.3
  145.2 129.8 all-gather.5
  277.8 167.2 all-gather.7
  472.6 10.3 reduce-scatter.1
where the time goes:
time: 493 us
  waiting for transfers between devices  402 us (82%)
  matrix products  49.8 us (10%)
  other arithmetic  19.2 us (4%)
  between operations  13.3 us (3%)
  starting transfers between devices  6.49 us (1%)
    all_gather x1, waiting for transfers between devices, body(): lax.all_gather(down_low, 'fs', axis=1, tiled=True)  147 us
    all_gather x1, waiting for transfers between devices, body(): lax.all_gather(gate_low, 'fs', axis=0, tiled=True)  128 us
    all_gather x1, waiting for transfers between devices, body(): lax.all_gather(value_low, 'fs', axis=0, tiled=True)  116 us
    dot_general x1, matrix products, body(): jnp.dot(hidden, down_full, preferred_element_type=jnp.float32)  27.4 us
    dot_general x1, matrix products, body(): value_raw = jnp.dot(normed, value_full, preferred_element_type=jnp.float32)  11.2 us
    dot_general x1, matrix products, body(): gate_raw = jnp.dot(normed, gate_full, preferred_element_type=jnp.float32)  11.1 us
    reduce_scatter x1, waiting for transfers between devices, body(): lax.psum_scatter(partial_terms.astype(jnp.bfloat16), 'tp', scatter_dimens...  10.5 us
  transfers between devices with their start and end apart: 6, of which 4 were waited for; matrix products, arithmetic and copies ran while one was open for 7% of the time, Pallas kernels for 0%

commit v1 on v0

--- a/solution.py
+++ b/solution.py
@@ -1,6 +1,11 @@
+import functools
+import math
+
 import jax
 import jax.numpy as jnp
 from jax import lax
+from jax.experimental import pallas as pl
+from jax.experimental.pallas import tpu as pltpu
 from jax.sharding import PartitionSpec as P
 
 epsilon = 1e-06
@@ -71,9 +76,454 @@
     return (summed * down_scale[None, :]).astype(jnp.bfloat16)
 
 
+MESH = pl.DeviceIdType.MESH
+GROUP = 4
+
+
+def fused_kernel(
+    depth_planes,
+    nrm,
+    wu,
+    wd,
+    par,
+    osc,
+    out,
+    tok,
+    up_all,
+    down_all,
+    hidden,
+    stage,
+    pair_in,
+    peer_in,
+    taps,
+    halo_out,
+    halo_in,
+    sem_local,
+    sem_plane_send,
+    sem_up_recv,
+    sem_down_recv,
+    sem_up_send,
+    sem_down_send,
+    sem_tok_send,
+    sem_tok_recv,
+    sem_tok_pair_send,
+    sem_tok_pair_recv,
+    sem_halo,
+    sem_pair_send,
+    sem_pair_recv,
+    sem_peer_send,
+    sem_peer_recv,
+):
+    planes = depth_planes
+    half = planes // 2
+    me = lax.axis_index("fs")
+    core = lax.axis_index("tp")
+    z, p = me // GROUP, me % GROUP
+    rows_own = nrm.shape[0]
+    part_rows = rows_own // 2
+    piece = wu.shape[1]
+    units = hidden.shape[1]
+    out_piece = wd.shape[2]
+    chunk = GROUP * out_piece
+    has_up, has_down = z < planes - 1, z > 0
+
+    def flip(mask):
+        px, py = p % 2, p // 2
+        if mask & 1:
+            px = 1 - px
+        if mask & 2:
+            py = 1 - py
+        return py * 2 + px
+
+    def chip(target):
+        return (z * GROUP + target, core)
+
+    others = (1, 2, 3)
+
+    barrier = pltpu.get_barrier_semaphore()
+    for mask in others:
+        pl.semaphore_signal(barrier, inc=1, device_id=chip(flip(mask)), device_id_type=MESH)
+    pl.semaphore_signal(barrier, inc=1, device_id=(me, 1 - core), device_id_type=MESH)
+
+    @pl.when(has_up)
+    def _():
+        pl.semaphore_signal(barrier, inc=1, device_id=(me + GROUP, core), device_id_type=MESH)
+
+    @pl.when(has_down)
+    def _():
+        pl.semaphore_signal(barrier, inc=1, device_id=(me - GROUP, core), device_id_type=MESH)
+
+    pl.semaphore_wait(barrier, 4 + has_up.astype(jnp.int32) + has_down.astype(jnp.int32))
+
+    def up_block(f):
+        return up_all.at[pl.ds(pl.multiple_of(f * piece, piece), piece), :]
+
+    def down_block(f):
+        return down_all.at[:, pl.ds(pl.multiple_of(f * out_piece, out_piece), out_piece)]
+
+    def remote(src, dst, send, recv, device):
+        return pltpu.make_async_remote_copy(
+            src_ref=src, dst_ref=dst, send_sem=send, recv_sem=recv, device_id=device, device_id_type=MESH
+        )
+
+    def plane_copy(kind, mask):
+        target = flip(mask)
+        src, block, recv = ((wu, up_block, sem_up_recv), (wd, down_block, sem_down_recv))[kind]
+        return remote(src.at[target], block(me), sem_plane_send.at[kind, mask], recv.at[me], chip(target))
+
+    def line_copy(kind, direction, f):
+        block, send, recv = (
+            (up_block, sem_up_send, sem_up_recv),
+            (down_block, sem_down_send, sem_down_recv),
+        )[kind]
+        step = GROUP if direction == 0 else -GROUP
+        return remote(block(f), block(f), send.at[direction, f], recv.at[f], (me + step, core))
+
+    def wait_piece(kind, f):
+        block, send, recv = (
+            (up_block, sem_up_send, sem_up_recv),
+            (down_block, sem_down_send, sem_down_recv),
+        )[kind]
+        remote(block(f), block(f), send.at[0, f], recv.at[f], (me, 1 - core)).wait_recv()
+
+    def forward(kind, direction, f):
+        @pl.when(has_up if direction == 0 else has_down)
+        def _():
+            line_copy(kind, direction, f).start()
+
+    def token_rows(owner, part):
+        start = pl.multiple_of(owner * rows_own + part * part_rows, part_rows)
+        return tok.at[pl.ds(start, part_rows), :]
+
+    def token_copy(mask):
+        start = pl.multiple_of(core * part_rows, part_rows)
+        return remote(
+            nrm.at[pl.ds(start, part_rows), :],
+            token_rows(p, core),
+            sem_tok_send.at[mask],
+            sem_tok_recv.at[mask],
+            chip(flip(mask)),
+        )
+
+    def token_pair_copy(mask):
+        here = token_rows(flip(mask), core)
+        return remote(here, here, sem_tok_pair_send.at[mask], sem_tok_pair_recv.at[mask], (me, 1 - core))
+
+    own_up = pltpu.make_async_copy(wu.at[p], up_block(me), sem_local.at[0])
+    own_down = pltpu.make_async_copy(wd.at[p], down_block(me), sem_local.at[1])
+    own_tok = pltpu.make_async_copy(
+        nrm, tok.at[pl.ds(pl.multiple_of(p * rows_own, rows_own), rows_own), :], sem_local.at[2]
+    )
+    own_up.start()
+    own_down.start()
+    own_tok.start()
+    for kind in (0, 1):
+        for mask in others:
+            plane_copy(kind, mask).start()
+    for mask in others:
+        token_copy(mask).start()
+    own_up.wait()
+    for direction in (0, 1):
+        forward(0, direction, me)
+    own_down.wait()
+    own_tok.wait()
+    for mask in others:
+        f = z * GROUP + flip(mask)
+        wait_piece(0, f)
+        for direction in (0, 1):
+            forward(0, direction, f)
+
+    def plane_of(step):
+        distance = (step + 1) // 2
+        below = step % 2
+        return z + distance * (1 - 2 * below), below
+
+    def relay(kind, q, below):
+        def one(i, carry):
+            f = q * GROUP + i
+            wait_piece(kind, f)
+
+            @pl.when((below == 1) & has_up)
+            def _():
+                line_copy(kind, 0, f).start()
+
+            @pl.when((below == 0) & has_down)
+            def _():
+                line_copy(kind, 1, f).start()
+
+            return carry
+
+        lax.fori_loop(0, GROUP, one, 0)
+
+    def up_step(step, carry):
+        q, below = plane_of(step)
+
+        @pl.when((q >= 0) & (q < planes))
+        def _():
+            relay(0, q, below)
+
+        return carry
+
+    lax.fori_loop(1, 2 * planes - 1, up_step, 0)
+
+    for direction in (0, 1):
+        forward(1, direction, me)
+    for mask in others:
+        f = z * GROUP + flip(mask)
+        wait_piece(1, f)
+        for direction in (0, 1):
+            forward(1, direction, f)
+
+    def token_pair_wait(mask):
+        there = token_rows(flip(mask), 1 - core)
+        remote(there, there, sem_tok_pair_send.at[mask], sem_tok_pair_recv.at[mask], (me, 1 - core)).wait_recv()
+
+    for mask in others:
+        landed = token_rows(flip(mask), core)
+        remote(landed, landed, sem_tok_send.at[mask], sem_tok_recv.at[mask], (me, 1 - core)).wait_recv()
+        token_pair_copy(mask).start()
+    for mask in others:
+        token_pair_wait(mask)
+
+    all_rows = tok.shape[0]
+    columns = up_all.shape[1]
+    tile = taps.shape[0] - 8
+    halo_rows = halo_out.shape[0]
+
+    def wide(j):
+        return pl.ds(pl.multiple_of(j * 256, 256), 256)
+
+    def halo_step(j, carry):
+        raw = jnp.dot(tok[all_rows - halo_rows :, :], up_all[:, wide(j)], preferred_element_type=jnp.float32)
+        halo_out[:, wide(j)] = (raw * par[0:1, wide(j)]).astype(jnp.bfloat16)
+        return carry
+
+    lax.fori_loop(0, columns // 256, halo_step, 0)
+
+    halo_copy = remote(halo_out, halo_in, sem_halo.at[0], sem_halo.at[1], (me + GROUP, core))
+
+    @pl.when(has_up)
+    def _():
+        halo_copy.start()
+
+    @pl.when(has_down)
+    def _():
+        remote(halo_out, halo_in, sem_halo.at[0], sem_halo.at[1], (me, 1 - core)).wait_recv()
+
+    @pl.when(jnp.logical_not(has_down))
+    def _():
+        halo_in[...] = jnp.zeros_like(halo_in)
+
+    def column_step(j, carry):
+        taps[0:8, :] = halo_in[:, wide(j)].astype(jnp.float32)[halo_rows - 8 :, :]
+
+        def row_step(m, inner):
+            rows = pl.ds(pl.multiple_of(m * tile, tile), tile)
+            raw = jnp.dot(tok[rows, :], up_all[:, wide(j)], preferred_element_type=jnp.float32)
+            taps[8:, :] = (raw * par[0:1, wide(j)]).astype(jnp.bfloat16).astype(jnp.float32)
+            conv = par[4:5, wide(j)] + par[3:4, wide(j)] * taps[8 : 8 + tile, :]
+            conv = conv + par[2:3, wide(j)] * taps[7 : 7 + tile, :]
+            conv = conv + par[1:2, wide(j)] * taps[6 : 6 + tile, :]
+            g, v = conv[:, :128], conv[:, 128:]
+            act = 0.5 * g * (1.0 + jnp.tanh(math.sqrt(2.0 / math.pi) * (g + 0.044715 * (g * g * g))))
+            hidden[rows, pl.ds(pl.multiple_of(j * 128, 128), 128)] = (act * v).astype(jnp.bfloat16)
+            taps[0:8, :] = taps[tile : tile + 8, :]
+            return inner
+
+        return lax.fori_loop(0, all_rows // tile, row_step, carry)
+
+    lax.fori_loop(0, columns // 256, column_step, 0)
+
+    def block_rows(owner):
+        return pl.ds(pl.multiple_of(owner * rows_own, rows_own), rows_own)
+
+    def pair_copy(q, owner):
+        return remote(
+            stage.at[q, owner],
+            pair_in.at[q % half, owner],
+            sem_pair_send.at[q % half, owner],
+            sem_pair_recv.at[q % half, owner],
+            (me, 1 - core),
+        )
+
+    def peer_copy(q, mask):
+        return remote(
+            stage.at[q, flip(mask)],
+            peer_in.at[q % half, mask - 1],
+            sem_peer_send.at[q % half, mask],
+            sem_peer_recv.at[q % half, mask],
+            chip(flip(mask)),
+        )
+
+    def down_step(step, carry):
+        q, below = plane_of(step)
+
+        @pl.when((q >= 0) & (q < planes))
+        def _():
+            @pl.when(step > 0)
+            def _():
+                relay(1, q, below)
+
+            mine = q // half == core
+            cols = pl.ds(pl.multiple_of(q * chunk, chunk), chunk)
+
+            def product(owner, inner):
+                value = jnp.dot(hidden[block_rows(owner), :], down_all[:, cols], preferred_element_type=jnp.float32)
+                stage[q, owner] = value.astype(jnp.bfloat16)
+
+                @pl.when(jnp.logical_not(mine))
+                def _():
+                    pair_copy(q, owner).start()
+
+                return inner
+
+            lax.fori_loop(0, GROUP, product, 0)
+
+            @pl.when(mine)
+            def _():
+                def combine(owner):
+                    pair_copy(q, owner).wait_recv()
+                    both = stage[q, owner].astype(jnp.float32) + pair_in[q % half, owner].astype(jnp.float32)
+                    stage[q, owner] = both.astype(jnp.bfloat16)
+
+                for mask in (3, 1, 2):
+                    combine(flip(mask))
+                    peer_copy(q, mask).start()
+                combine(p)
+
+        return carry
+
+    lax.fori_loop(0, 2 * planes - 1, down_step, 0)
+
+    def finish(i, carry):
+        q = core * half + i
+        total = stage[q, p].astype(jnp.float32)
+        for mask in others:
+            peer_copy(q, mask).wait_recv()
+            total = total + peer_in[i, mask - 1].astype(jnp.float32)
+        cols = pl.ds(pl.multiple_of(i * chunk, chunk), chunk)
+        out[:, cols] = (total * osc[0:1, cols]).astype(jnp.bfloat16)
+        return carry
+
+    lax.fori_loop(0, half, finish, 0)
+
+    def drain_out(i, carry):
+        for mask in others:
+            peer_copy(core * half + i, mask).wait_send()
+
+        def one(owner, inner):
+            pair_copy((1 - core) * half + i, owner).wait_send()
+            return inner
+
+        return lax.fori_loop(0, GROUP, one, carry)
+
+    lax.fori_loop(0, half, drain_out, 0)
+    for mask in others:
+        token_copy(mask).wait_send()
+        token_pair_copy(mask).wait_send()
+        for kind in (0, 1):
+            plane_copy(kind, mask).wait_send()
+
+    @pl.when(has_up)
+    def _():
+        halo_copy.wait_send()
+
+    def drain_line(f, carry):
+        for kind in (0, 1):
+
+            @pl.when(has_up & (f // GROUP <= z))
+            def _():
+                line_copy(kind, 0, f).wait_send()
+
+            @pl.when(has_down & (f // GROUP >= z))
+            def _():
+                line_copy(kind, 1, f).wait_send()
+
+        return carry
+
+    lax.fori_loop(0, planes * GROUP, drain_line, 0)
+
+
+def grouped_body(count, tokens, norm_gain, gate_weight, value_weight, gate_scale, value_scale, gate_kernel, value_kernel, gate_bias, value_bias, down_weight, down_scale):
+    planes = count // GROUP
+    half = planes // 2
+    p = lax.axis_index("fs") % GROUP
+    normed = normalize(tokens, norm_gain)
+    rows, width = normed.shape
+    piece, local = gate_weight.shape
+    out_piece = down_weight.shape[1]
+    units = local // GROUP
+    blocks = units // 128
+    chunk = GROUP * out_piece
+    both = jnp.stack([gate_weight.astype(jnp.bfloat16), value_weight.astype(jnp.bfloat16)], axis=0)
+    both = both.reshape(2, piece, GROUP, blocks, 128).transpose(2, 1, 3, 0, 4)
+    wu = both.reshape(GROUP, piece, 2 * units)
+    wd = down_weight.astype(jnp.bfloat16).reshape(GROUP, units, out_piece)
+
+    def pick(gate, value):
+        gate = lax.dynamic_slice_in_dim(gate, p * units, units, axis=1)
+        value = lax.dynamic_slice_in_dim(value, p * units, units, axis=1)
+        n = gate.shape[0]
+        pair = jnp.stack([gate.reshape(n, blocks, 128), value.reshape(n, blocks, 128)], axis=2)
+        return pair.reshape(n, 2 * units)
+
+    gate_rows = jnp.concatenate([gate_scale[None], gate_kernel, gate_bias[None], jnp.zeros((3, local), jnp.float32)], axis=0)
+    value_rows = jnp.concatenate([value_scale[None], value_kernel, value_bias[None], jnp.zeros((3, local), jnp.float32)], axis=0)
+    par = pick(gate_rows, value_rows)
+    tile = rows // 2
+    dma = pltpu.SemaphoreType.DMA
+    bf16 = jnp.bfloat16
+    vmem = pl.BlockSpec(memory_space=pltpu.VMEM)
+    return pl.pallas_call(
+        functools.partial(fused_kernel, planes),
+        out_shape=jax.ShapeDtypeStruct((rows, half * chunk), bf16),
+        in_specs=[vmem] * 5,
+        out_specs=vmem,
+        scratch_shapes=[
+            pltpu.VMEM((GROUP * rows, width), bf16),
+            pltpu.VMEM((width, 2 * units), bf16),
+            pltpu.VMEM((units, width), bf16),
+            pltpu.VMEM((GROUP * rows, units), bf16),
+            pltpu.VMEM((planes, GROUP, rows, chunk), bf16),
+            pltpu.VMEM((half, GROUP, rows, chunk), bf16),
+            pltpu.VMEM((half, GROUP - 1, rows, chunk), bf16),
+            pltpu.VMEM((tile + 8, 256), jnp.float32),
+            pltpu.VMEM((16, 2 * units), bf16),
+            pltpu.VMEM((16, 2 * units), bf16),
+            dma((3,)),
+            dma((2, GROUP)),
+            dma((count,)),
+            dma((count,)),
+            dma((2, count)),
+            dma((2, count)),
+            dma((GROUP,)),
+            dma((GROUP,)),
+            dma((GROUP,)),
+            dma((GROUP,)),
+            dma((2,)),
+            dma((half, GROUP)),
+            dma((half, GROUP)),
+            dma((half, GROUP)),
+            dma((half, GROUP)),
+        ],
+        compiler_params=pltpu.CompilerParams(
+            collective_id=0, has_side_effects=True, vmem_limit_bytes=67043328
+        ),
+    )(normed, wu, wd, par, down_scale[None, :])
+
+
 def solution(mesh):
+    count, tp = mesh.shape["fs"], mesh.shape["tp"]
+
+    def whole(*arrays):
+        local = arrays[2].shape[1]
+        fits = tp == 2 and count % (2 * GROUP) == 0 and local % (GROUP * 128) == 0
+        if fits:
+            return grouped_body(count, *arrays)
+        return body(*arrays)
+
     return jax.shard_map(
-        body,
+        whole,
         mesh=mesh,
         in_specs=(
             P("fs", None),

time: 493 us -> 237 us (0.48)
  waiting for transfers between devices: 402 us -> 0 us
  Pallas kernels: 0 us -> 213 us
  matrix products: 49.8 us -> 0 us
  between operations: 13.3 us -> 0.2 us
  local copies, waits for them, and re-layouts: 2.08 us -> 12.2 us
  other arithmetic: 19.2 us -> 9.27 us
  starting transfers between devices: 6.49 us -> 0 us
    all_gather x3 -> x0, waiting for transfers between devices: 391 us -> none  [the longest x1 147 us: body(): lax.all_gather(down_low, 'fs', axis=1, tiled=True)]
    pallas_call x0 -> x1, Pallas kernels: none -> 213 us  [grouped_body(): pl.pallas_call(functools.partial(fused_kernel, planes), out_shape=jax.Sha...]
    dot_general x3 -> x0, matrix products: 49.8 us -> none  [the longest x1 27.4 us: body(): jnp.dot(hidden, down_full, preferred_element_type=jnp.float32)]
    convert_element_type x6 -> x2, other arithmetic: 18.5 us -> 4.65 us  [the longest x1 2.42 us: normalize(): return (scaled * norm_gain[None, :]).astype(jnp.bfloat16)]
    reduce_scatter x1 -> x0, waiting for transfers between devices: 10.5 us -> none  [body(): lax.psum_scatter(partial_terms.astype(jnp.bfloat16), 'tp', scatter_dimens...]
    ppermute x2 -> x0, starting transfers between devices: 6.32 us -> none  [from_behind(): lax.ppermute(value, axis, [(source, source + steps) for source in range(l...]
  transfers between devices with their start and end apart: 6 -> 0, of which waited for: 4 -> 0; matrix products, arithmetic and copies ran while one was open for 7% -> 0% of each run, Pallas kernels for 0% -> 0%
where the time goes in v1:
time: 237 us; the launch traced here: 235 us
  Pallas kernels  213 us (90%)
  local copies, waits for them, and re-layouts  12.2 us (5%)
  other arithmetic  9.27 us (4%)
    pallas_call x1, Pallas kernels, grouped_body(): pl.pallas_call(functools.partial(fused_kernel, planes), out_shape=jax.Sha...  213 us

profile of v1, /device:TPU:1, one launch (start us, length us, event | category | flops | bytes accessed | tf_op | source)
XLA Modules:
  0.0 234.6 jit_solution(8880746887935254131)
XLA Ops:
  0.0 0.0 copy-start.8
  0.0 0.0 copy-start.7
  0.0 0.0 copy-start.4
  0.0 0.0 copy-start.3
  0.0 0.0 copy-start.6
  0.0 0.0 copy-start.5
  0.0 0.0 copy-start.2
  0.0 0.0 copy-start.1
  0.1 0.1 pad.9.clone
  0.2 2.7 %fusion = f32[768]{0:T(1024)S(1)} fusion(bf16[768,2048]{1,0:T(8,128)(2,1)} %param.12), kind=kLoop, calls=%fused_computation.2 | loop fusion | flops 4717824 | bytes 3148800 | tf_op jit(solution)/shard_map/reduce_sum | solution.py:22
  2.9 0.0 copy-done.5
  2.9 0.0 copy-done.6
  3.0 0.0 copy-done.7
  3.0 0.0 copy-done.8
  3.0 0.0 copy-done.4
  3.0 0.0 copy-done.3
  3.0 0.1 fusion.10
  3.1 0.6 pad_maximum_fusion
  3.8 0.0 copy-done.1
  3.8 0.3 copy.15
  4.1 0.0 copy-done.2
  4.1 0.3 copy.16
  4.4 1.2 maximum_bitcast_fusion
  5.6 0.0 copy-start
  5.6 0.0 copy-start.9
  5.6 4.5 %copy.17 = bf16[4,128,5,2,128]{4,3,2,1,0:T(2,128)(2,1)} copy(bf16[4,128,5,2,128]{1,4,2,0,3:T(8,128)(2,1)} %maximum_bitcast_fusion) | data formatting | bytes 2621440 | tf_op jit(solution)/shard_map/transpose | solution.py:459
  10.1 4.2 %reshape.23.wu = bf16[4,128,1280]{2,1,0:T(8,128)(2,1)} reshape(bf16[4,128,5,2,128]{4,3,2,1,0:T(2,128)(2,1)} %copy.17) | data formatting | bytes 2621440 | tf_op jit(solution)/shard_map/reshape | solution.py:460
  14.3 2.2 convert_element_type.19
  16.5 0.0 copy-done
  16.5 0.0 copy-done.9
  16.6 2.4 %fusion.2.nrm = bf16[768,2048]{1,0:T(8,128)(2,1)} fusion(bf16[768,2048]{1,0:T(8,128)(2,1)S(1)} %copy-done, f32[2048]{0:T(1024)S(1)} %copy-done.9, f32[768]{0:T(1024)S(1)} %add_rsqrt_fusion), kind=kLoop, calls=%fused_computation.4 | loop fusion | flops 6291456 | bytes 6302720 | tf_op jit(solution)/shard_map/convert_element_type | solution.py:23
  19.0 212.9 %shard_map.118 = bf16[768,1024]{1,0:T(8,128)(2,1)} custom-call(bf16[768,2048]{1,0:T(8,128)(2,1)} %fusion.2.nrm, bf16[4,128,1280]{2,1,0:T(8,128)(2,1)} %reshape.23.wu, bf16[4,640,128]{2,1,0:T(8,128)(2,1)} %bitcast.11, f32[8,1280]{1,0:T(8,128)} %bitcast.14, f32[1,1024]{1,0:T(1,128)} %bitcast.15), custom_call_target="tpu_custom_call" | custom-call | tf_op jit(solution)/shard_map/pallas_call | solution.py:477
  231.9 2.7 %copy.19 = bf16[768,1024]{1,0:T(8,128)(2,1)} copy(bf16[768,1024]{1,0:T(8,128)(2,1)} %shard_map.118) | data formatting | bytes 3145728
  (6 shorter events, 0.0 us)
Async XLA Ops:
  0.0 3.0 %copy-start.8 = (f32[2560]{0:T(1024)S(1)}, f32[2560]{0:T(1024)}, u32[]{:S(2)}) copy-start(f32[2560]{0:T(1024)} %param.21) | copy-start | bytes 30724
  0.0 2.9 %copy-start.7 = (f32[2560]{0:T(1024)S(1)}, f32[2560]{0:T(1024)}, u32[]{:S(2)}) copy-start(f32[2560]{0:T(1024)} %param.20) | copy-start | bytes 30724
  0.0 3.0 %copy-start.4 = (f32[3,2560]{1,0:T(4,128)S(1)}, f32[3,2560]{1,0:T(4,128)}, u32[]{:S(2)}) copy-start(f32[3,2560]{1,0:T(4,128)} %param.19) | copy-start | bytes 92164
  0.0 3.0 %copy-start.3 = (f32[3,2560]{1,0:T(4,128)S(1)}, f32[3,2560]{1,0:T(4,128)}, u32[]{:S(2)}) copy-start(f32[3,2560]{1,0:T(4,128)} %param.18) | copy-start | bytes 92164
  0.0 2.9 %copy-start.6 = (f32[2560]{0:T(1024)S(1)}, f32[2560]{0:T(1024)}, u32[]{:S(2)}) copy-start(f32[2560]{0:T(1024)} %param.17) | copy-start | bytes 30724
  0.0 2.9 %copy-start.5 = (f32[2560]{0:T(1024)S(1)}, f32[2560]{0:T(1024)}, u32[]{:S(2)}) copy-start(f32[2560]{0:T(1024)} %param.16) | copy-start | bytes 30724
  0.0 4.0 %copy-start.2 = (f32[128,2560]{1,0:T(8,128)S(1)}, f32[128,2560]{1,0:T(8,128)}, u32[]{:S(2)}) copy-start(f32[128,2560]{1,0:T(8,128)} %param.15) | copy-start | bytes 3932164
  0.0 3.7 %copy-start.1 = (f32[128,2560]{1,0:T(8,128)S(1)}, f32[128,2560]{1,0:T(8,128)}, u32[]{:S(2)}) copy-start(f32[128,2560]{1,0:T(8,128)} %param.14) | copy-start | bytes 3932164
  5.6 11.0 %copy-start = (bf16[768,2048]{1,0:T(8,128)(2,1)S(1)}, bf16[768,2048]{1,0:T(8,128)(2,1)}, u32[]{:S(2)}) copy-start(bf16[768,2048]{1,0:T(8,128)(2,1)} %param.12) | copy-start | bytes 9437188
  5.6 11.0 %copy-start.9 = (f32[2048]{0:T(1024)S(1)}, f32[2048]{0:T(1024)}, u32[]{:S(2)}) copy-start(f32[2048]{0:T(1024)} %param.13) | copy-start | bytes 24580

commit v2 on v1

--- a/solution.py
+++ b/solution.py
@@ -82,10 +82,17 @@
 
 def fused_kernel(
     depth_planes,
-    nrm,
-    wu,
-    wd,
-    par,
+    tok_hbm,
+    gate_hbm,
+    value_hbm,
+    down_hbm,
+    gain,
+    gate_scale,
+    value_scale,
+    gate_kernel,
+    value_kernel,
+    gate_bias,
+    value_bias,
     osc,
     out,
     tok,
@@ -95,9 +102,17 @@
     stage,
     pair_in,
     peer_in,
+    relay_in,
     taps,
     halo_out,
     halo_in,
+    par,
+    wu,
+    wd,
+    raw_tok,
+    raw_gate,
+    raw_value,
+    raw_down,
     sem_local,
     sem_plane_send,
     sem_up_recv,
@@ -113,13 +128,17 @@
     sem_pair_recv,
     sem_peer_send,
     sem_peer_recv,
+    sem_relay_send,
+    sem_relay_recv,
+    sem_late_recv,
+    sem_late_send,
 ):
     planes = depth_planes
     half = planes // 2
     me = lax.axis_index("fs")
     core = lax.axis_index("tp")
     z, p = me // GROUP, me % GROUP
-    rows_own = nrm.shape[0]
+    rows_own = raw_tok.shape[0]
     part_rows = rows_own // 2
     piece = wu.shape[1]
     units = hidden.shape[1]
@@ -140,6 +159,15 @@
 
     others = (1, 2, 3)
 
+    fetches = [
+        pltpu.make_async_copy(src, dst, sem_local.at[2 + i])
+        for i, (src, dst) in enumerate(
+            ((gate_hbm, raw_gate), (value_hbm, raw_value), (down_hbm, raw_down), (tok_hbm, raw_tok))
+        )
+    ]
+    for fetch in fetches:
+        fetch.start()
+
     barrier = pltpu.get_barrier_semaphore()
     for mask in others:
         pl.semaphore_signal(barrier, inc=1, device_id=chip(flip(mask)), device_id_type=MESH)
@@ -153,13 +181,48 @@
     def _():
         pl.semaphore_signal(barrier, inc=1, device_id=(me - GROUP, core), device_id_type=MESH)
 
+    blocks = units // 128
+    fetches[0].wait()
+    fetches[1].wait()
+    for m in range(GROUP):
+        for j in range(blocks):
+            first = (m * blocks + j) * 128
+            wu[m, :, j * 256 : j * 256 + 128] = raw_gate[:, first : first + 128].astype(jnp.bfloat16)
+            wu[m, :, j * 256 + 128 : j * 256 + 256] = raw_value[:, first : first + 128].astype(jnp.bfloat16)
+    fetches[2].wait()
+    for m in range(GROUP):
+        wd[m] = raw_down[m * units : (m + 1) * units, :].astype(jnp.bfloat16)
+    for j in range(blocks):
+        src = pl.ds(pl.multiple_of(p * units + j * 128, 128), 128)
+        for side, (scale, kernel, tap_bias) in enumerate(
+            ((gate_scale, gate_kernel, gate_bias), (value_scale, value_kernel, value_bias))
+        ):
+            dst = slice(j * 256 + side * 128, j * 256 + side * 128 + 128)
+            par[0:1, dst] = scale[0:1, src]
+            par[1:4, dst] = kernel[0:3, src]
+            par[4:5, dst] = tap_bias[0:1, src]
     pl.semaphore_wait(barrier, 4 + has_up.astype(jnp.int32) + has_down.astype(jnp.int32))
 
+    early = (blocks + 1) // 2 * 256
+    columns = up_all.shape[1]
+
+    def up_whole(f):
+        return up_all.at[pl.ds(pl.multiple_of(f * piece, piece), piece), :]
+
     def up_block(f):
-        return up_all.at[pl.ds(pl.multiple_of(f * piece, piece), piece), :]
+        return up_all.at[pl.ds(pl.multiple_of(f * piece, piece), piece), 0:early]
+
+    def late_block(f):
+        return up_all.at[pl.ds(pl.multiple_of(f * piece, piece), piece), early:columns]
 
     def down_block(f):
         return down_all.at[:, pl.ds(pl.multiple_of(f * out_piece, out_piece), out_piece)]
+
+    kinds = (
+        (up_block, sem_up_send, sem_up_recv),
+        (down_block, sem_down_send, sem_down_recv),
+        (late_block, sem_late_send, sem_late_recv),
+    )
 
     def remote(src, dst, send, recv, device):
         return pltpu.make_async_remote_copy(
@@ -168,22 +231,17 @@
 
     def plane_copy(kind, mask):
         target = flip(mask)
-        src, block, recv = ((wu, up_block, sem_up_recv), (wd, down_block, sem_down_recv))[kind]
-        return remote(src.at[target], block(me), sem_plane_send.at[kind, mask], recv.at[me], chip(target))
+        block, _, recv = kinds[kind]
+        src = (wu.at[target, :, 0:early], wd.at[target], wu.at[target, :, early:columns])[kind]
+        return remote(src, block(me), sem_plane_send.at[kind, mask], recv.at[me], chip(target))
 
     def line_copy(kind, direction, f):
-        block, send, recv = (
-            (up_block, sem_up_send, sem_up_recv),
-            (down_block, sem_down_send, sem_down_recv),
-        )[kind]
+        block, send, recv = kinds[kind]
         step = GROUP if direction == 0 else -GROUP
         return remote(block(f), block(f), send.at[direction, f], recv.at[f], (me + step, core))
 
     def wait_piece(kind, f):
-        block, send, recv = (
-            (up_block, sem_up_send, sem_up_recv),
-            (down_block, sem_down_send, sem_down_recv),
-        )[kind]
+        block, send, recv = kinds[kind]
         remote(block(f), block(f), send.at[0, f], recv.at[f], (me, 1 - core)).wait_recv()
 
     def forward(kind, direction, f):
@@ -196,61 +254,86 @@
         return tok.at[pl.ds(start, part_rows), :]
 
     def token_copy(mask):
-        start = pl.multiple_of(core * part_rows, part_rows)
-        return remote(
-            nrm.at[pl.ds(start, part_rows), :],
-            token_rows(p, core),
-            sem_tok_send.at[mask],
-            sem_tok_recv.at[mask],
-            chip(flip(mask)),
-        )
+        here = token_rows(p, core)
+        return remote(here, here, sem_tok_send.at[mask], sem_tok_recv.at[mask], chip(flip(mask)))
+
+    quarter = part_rows // 2
+
+    def token_quarter(owner, which):
+        start = owner * rows_own + core * part_rows + which * quarter
+        return tok.at[pl.ds(pl.multiple_of(start, quarter), quarter), :]
+
+    def token_relay(mask):
+        which = mask - 1
+        slot = (3, 0)[which]
+        here = token_quarter(flip(mask), which)
+        return remote(here, here, sem_tok_send.at[slot], sem_tok_recv.at[slot], chip(flip(3 - mask)))
 
     def token_pair_copy(mask):
         here = token_rows(flip(mask), core)
         return remote(here, here, sem_tok_pair_send.at[mask], sem_tok_pair_recv.at[mask], (me, 1 - core))
 
-    own_up = pltpu.make_async_copy(wu.at[p], up_block(me), sem_local.at[0])
+    own_up = pltpu.make_async_copy(wu.at[p], up_whole(me), sem_local.at[0])
     own_down = pltpu.make_async_copy(wd.at[p], down_block(me), sem_local.at[1])
-    own_tok = pltpu.make_async_copy(
-        nrm, tok.at[pl.ds(pl.multiple_of(p * rows_own, rows_own), rows_own), :], sem_local.at[2]
-    )
     own_up.start()
     own_down.start()
-    own_tok.start()
-    for kind in (0, 1):
+    for kind in (0, 2):
         for mask in others:
             plane_copy(kind, mask).start()
-    for mask in others:
-        token_copy(mask).start()
     own_up.wait()
     for direction in (0, 1):
         forward(0, direction, me)
+
+    fetches[3].wait()
+    norm_tile = 64
+
+    def norm_step(i, carry):
+        first = pl.multiple_of(i * norm_tile, norm_tile)
+        values = raw_tok[pl.ds(first, norm_tile), :].astype(jnp.float32)
+        scaled = values * lax.rsqrt(jnp.mean(values * values, axis=1, keepdims=True) + epsilon)
+        rows = pl.ds(pl.multiple_of(p * rows_own + i * norm_tile, norm_tile), norm_tile)
+        tok[rows, :] = (scaled * gain[...]).astype(jnp.bfloat16)
+        return carry
+
+    lax.fori_loop(0, rows_own // norm_tile, norm_step, 0)
     own_down.wait()
-    own_tok.wait()
+
+    def own_plane(kind):
+        for mask in others:
+            f = z * GROUP + flip(mask)
+            wait_piece(kind, f)
+            for direction in (0, 1):
+                forward(kind, direction, f)
+
+    own_plane(0)
+    for mask in (1, 2):
+        token_copy(mask).start()
     for mask in others:
-        f = z * GROUP + flip(mask)
-        wait_piece(0, f)
-        for direction in (0, 1):
-            forward(0, direction, f)
+        plane_copy(1, mask).start()
+    for direction in (0, 1):
+        forward(2, direction, me)
+    own_plane(2)
 
     def plane_of(step):
         distance = (step + 1) // 2
         below = step % 2
         return z + distance * (1 - 2 * below), below
 
+    def relay_one(kind, q, below, i):
+        f = q * GROUP + i
+        wait_piece(kind, f)
+
+        @pl.when((below == 1) & has_up)
+        def _():
+            line_copy(kind, 0, f).start()
+
+        @pl.when((below == 0) & has_down)
+        def _():
+            line_copy(kind, 1, f).start()
+
     def relay(kind, q, below):
         def one(i, carry):
-            f = q * GROUP + i
-            wait_piece(kind, f)
-
-            @pl.when((below == 1) & has_up)
-            def _():
-                line_copy(kind, 0, f).start()
-
-            @pl.when((below == 0) & has_down)
-            def _():
-                line_copy(kind, 1, f).start()
-
+            relay_one(kind, q, below, i)
             return carry
 
         lax.fori_loop(0, GROUP, one, 0)
@@ -264,29 +347,32 @@
 
         return carry
 
-    lax.fori_loop(1, 2 * planes - 1, up_step, 0)
-
-    for direction in (0, 1):
-        forward(1, direction, me)
-    for mask in others:
-        f = z * GROUP + flip(mask)
-        wait_piece(1, f)
-        for direction in (0, 1):
-            forward(1, direction, f)
+    lax.fori_loop(1, 2 * planes - 3, up_step, 0)
+
+    def token_wait(mask):
+        landed = token_rows(flip(mask), core)
+        remote(landed, landed, sem_tok_send.at[mask], sem_tok_recv.at[mask], (me, 1 - core)).wait_recv()
+
+    for mask in (1, 2):
+        token_wait(mask)
+        token_relay(mask).start()
+        token_pair_copy(mask).start()
+
+    lax.fori_loop(2 * planes - 3, 2 * planes - 1, up_step, 0)
 
     def token_pair_wait(mask):
         there = token_rows(flip(mask), 1 - core)
         remote(there, there, sem_tok_pair_send.at[mask], sem_tok_pair_recv.at[mask], (me, 1 - core)).wait_recv()
 
-    for mask in others:
-        landed = token_rows(flip(mask), core)
-        remote(landed, landed, sem_tok_send.at[mask], sem_tok_recv.at[mask], (me, 1 - core)).wait_recv()
-        token_pair_copy(mask).start()
+    for which in (0, 1):
+        slot = (3, 0)[which]
+        landed = token_quarter(flip(3), which)
+        remote(landed, landed, sem_tok_send.at[slot], sem_tok_recv.at[slot], (me, 1 - core)).wait_recv()
+    token_pair_copy(3).start()
     for mask in others:
         token_pair_wait(mask)
 
     all_rows = tok.shape[0]
-    columns = up_all.shape[1]
     tile = taps.shape[0] - 8
     halo_rows = halo_out.shape[0]
 
@@ -298,21 +384,37 @@
         halo_out[:, wide(j)] = (raw * par[0:1, wide(j)]).astype(jnp.bfloat16)
         return carry
 
-    lax.fori_loop(0, columns // 256, halo_step, 0)
-
-    halo_copy = remote(halo_out, halo_in, sem_halo.at[0], sem_halo.at[1], (me + GROUP, core))
-
-    @pl.when(has_up)
-    def _():
-        halo_copy.start()
-
-    @pl.when(has_down)
-    def _():
-        remote(halo_out, halo_in, sem_halo.at[0], sem_halo.at[1], (me, 1 - core)).wait_recv()
+    def halo_copy(part):
+        cols = (slice(0, early), slice(early, columns))[part]
+        here, there = halo_out.at[:, cols], halo_in.at[:, cols]
+        return remote(here, there, sem_halo.at[part], sem_halo.at[2 + part], (me + GROUP, core))
+
+    def halo_part(part, first, last):
+        lax.fori_loop(first, last, halo_step, 0)
+
+        @pl.when(has_up)
+        def _():
+            halo_copy(part).start()
+
+        @pl.when(has_down)
+        def _():
+            cols = (slice(0, early), slice(early, columns))[part]
+            here = halo_in.at[:, cols]
+            remote(here, here, sem_halo.at[part], sem_halo.at[2 + part], (me, 1 - core)).wait_recv()
 
     @pl.when(jnp.logical_not(has_down))
     def _():
         halo_in[...] = jnp.zeros_like(halo_in)
+
+    tiles = all_rows // tile
+    slots = (2 * planes - 2) * GROUP
+
+    def late_slot(slot):
+        q, below = plane_of(slot // GROUP + 1)
+
+        @pl.when((q >= 0) & (q < planes))
+        def _():
+            relay_one(2, q, below, slot % GROUP)
 
     def column_step(j, carry):
         taps[0:8, :] = halo_in[:, wide(j)].astype(jnp.float32)[halo_rows - 8 :, :]
@@ -328,11 +430,32 @@
             act = 0.5 * g * (1.0 + jnp.tanh(math.sqrt(2.0 / math.pi) * (g + 0.044715 * (g * g * g))))
             hidden[rows, pl.ds(pl.multiple_of(j * 128, 128), 128)] = (act * v).astype(jnp.bfloat16)
             taps[0:8, :] = taps[tile : tile + 8, :]
+            slot = j * tiles + m
+
+            @pl.when((slot < slots) & (j < early // 256))
+            def _():
+                late_slot(slot)
+
             return inner
 
-        return lax.fori_loop(0, all_rows // tile, row_step, carry)
-
-    lax.fori_loop(0, columns // 256, column_step, 0)
+        return lax.fori_loop(0, tiles, row_step, carry)
+
+    early_blocks = early // 256
+    halo_part(0, 0, early_blocks)
+    lax.fori_loop(0, early_blocks, column_step, 0)
+
+    def late_rest(slot, carry):
+        late_slot(slot)
+        return carry
+
+    if early_blocks * tiles < slots:
+        lax.fori_loop(early_blocks * tiles, slots, late_rest, 0)
+    for direction in (0, 1):
+        forward(1, direction, me)
+    own_plane(1)
+    if early_blocks < blocks:
+        halo_part(1, early_blocks, blocks)
+        lax.fori_loop(early_blocks, blocks, column_step, 0)
 
     def block_rows(owner):
         return pl.ds(pl.multiple_of(owner * rows_own, rows_own), rows_own)
@@ -346,12 +469,27 @@
             (me, 1 - core),
         )
 
-    def peer_copy(q, mask):
+    half_rows = rows_own // 2
+
+    def half_of(which):
+        return pl.ds(which * half_rows, half_rows)
+
+    def peer_copy(q, mask, which):
+        slot = (mask - 1) * 2 + which
         return remote(
-            stage.at[q, flip(mask)],
-            peer_in.at[q % half, mask - 1],
-            sem_peer_send.at[q % half, mask],
-            sem_peer_recv.at[q % half, mask],
+            stage.at[q, flip(mask), half_of(which)],
+            peer_in.at[q % half, mask - 1, half_of(which)],
+            sem_peer_send.at[q % half, slot],
+            sem_peer_recv.at[q % half, slot],
+            chip(flip(mask)),
+        )
+
+    def relay_copy(q, mask):
+        return remote(
+            stage.at[q, flip(3), half_of(mask - 1)],
+            relay_in.at[q % half, mask - 1],
+            sem_relay_send.at[q % half, mask - 1],
+            sem_relay_recv.at[q % half, mask - 1],
             chip(flip(mask)),
         )
 
@@ -386,10 +524,20 @@
                     both = stage[q, owner].astype(jnp.float32) + pair_in[q % half, owner].astype(jnp.float32)
                     stage[q, owner] = both.astype(jnp.bfloat16)
 
-                for mask in (3, 1, 2):
+                combine(flip(3))
+                for mask in (1, 2):
+                    relay_copy(q, mask).start()
+                for mask in (1, 2):
                     combine(flip(mask))
-                    peer_copy(q, mask).start()
+                    peer_copy(q, mask, mask - 1).start()
                 combine(p)
+                for mask in (1, 2):
+                    relay_copy(q, mask).wait_recv()
+                    owner = flip(3 - mask)
+                    rows = half_of(mask - 1)
+                    total = stage[q, owner, rows, :].astype(jnp.float32) + relay_in[q % half, mask - 1].astype(jnp.float32)
+                    stage[q, owner, rows, :] = total.astype(jnp.bfloat16)
+                    peer_copy(q, 3 - mask, mask - 1).start()
 
         return carry
 
@@ -398,8 +546,9 @@
     def finish(i, carry):
         q = core * half + i
         total = stage[q, p].astype(jnp.float32)
-        for mask in others:
-            peer_copy(q, mask).wait_recv()
+        for mask in (1, 2):
+            for which in (0, 1):
+                peer_copy(q, mask, which).wait_recv()
             total = total + peer_in[i, mask - 1].astype(jnp.float32)
         cols = pl.ds(pl.multiple_of(i * chunk, chunk), chunk)
         out[:, cols] = (total * osc[0:1, cols]).astype(jnp.bfloat16)
@@ -408,8 +557,10 @@
     lax.fori_loop(0, half, finish, 0)
 
     def drain_out(i, carry):
-        for mask in others:
-            peer_copy(core * half + i, mask).wait_send()
+        for mask in (1, 2):
+            relay_copy(core * half + i, mask).wait_send()
+            for which in (0, 1):
+                peer_copy(core * half + i, mask, which).wait_send()
 
         def one(owner, inner):
             pair_copy((1 - core) * half + i, owner).wait_send()
@@ -418,18 +569,22 @@
         return lax.fori_loop(0, GROUP, one, carry)
 
     lax.fori_loop(0, half, drain_out, 0)
+    for mask in (1, 2):
+        token_copy(mask).wait_send()
+        token_relay(mask).wait_send()
     for mask in others:
-        token_copy(mask).wait_send()
         token_pair_copy(mask).wait_send()
-        for kind in (0, 1):
+        for kind in (0, 1, 2):
             plane_copy(kind, mask).wait_send()
 
     @pl.when(has_up)
     def _():
-        halo_copy.wait_send()
+        halo_copy(0).wait_send()
+        if early < columns:
+            halo_copy(1).wait_send()
 
     def drain_line(f, carry):
-        for kind in (0, 1):
+        for kind in (0, 1, 2):
 
             @pl.when(has_up & (f // GROUP <= z))
             def _():
@@ -447,37 +602,20 @@
 def grouped_body(count, tokens, norm_gain, gate_weight, value_weight, gate_scale, value_scale, gate_kernel, value_kernel, gate_bias, value_bias, down_weight, down_scale):
     planes = count // GROUP
     half = planes // 2
-    p = lax.axis_index("fs") % GROUP
-    normed = normalize(tokens, norm_gain)
-    rows, width = normed.shape
+    rows, width = tokens.shape
     piece, local = gate_weight.shape
     out_piece = down_weight.shape[1]
     units = local // GROUP
-    blocks = units // 128
     chunk = GROUP * out_piece
-    both = jnp.stack([gate_weight.astype(jnp.bfloat16), value_weight.astype(jnp.bfloat16)], axis=0)
-    both = both.reshape(2, piece, GROUP, blocks, 128).transpose(2, 1, 3, 0, 4)
-    wu = both.reshape(GROUP, piece, 2 * units)
-    wd = down_weight.astype(jnp.bfloat16).reshape(GROUP, units, out_piece)
-
-    def pick(gate, value):
-        gate = lax.dynamic_slice_in_dim(gate, p * units, units, axis=1)
-        value = lax.dynamic_slice_in_dim(value, p * units, units, axis=1)
-        n = gate.shape[0]
-        pair = jnp.stack([gate.reshape(n, blocks, 128), value.reshape(n, blocks, 128)], axis=2)
-        return pair.reshape(n, 2 * units)
-
-    gate_rows = jnp.concatenate([gate_scale[None], gate_kernel, gate_bias[None], jnp.zeros((3, local), jnp.float32)], axis=0)
-    value_rows = jnp.concatenate([value_scale[None], value_kernel, value_bias[None], jnp.zeros((3, local), jnp.float32)], axis=0)
-    par = pick(gate_rows, value_rows)
     tile = rows // 2
     dma = pltpu.SemaphoreType.DMA
-    bf16 = jnp.bfloat16
+    bf16, f32 = jnp.bfloat16, jnp.float32
     vmem = pl.BlockSpec(memory_space=pltpu.VMEM)
+    hbm = pl.BlockSpec(memory_space=pl.ANY)
     return pl.pallas_call(
         functools.partial(fused_kernel, planes),
         out_shape=jax.ShapeDtypeStruct((rows, half * chunk), bf16),
-        in_specs=[vmem] * 5,
+        in_specs=[hbm] * 4 + [vmem] * 8,
         out_specs=vmem,
         scratch_shapes=[
             pltpu.VMEM((GROUP * rows, width), bf16),
@@ -486,12 +624,20 @@
             pltpu.VMEM((GROUP * rows, units), bf16),
             pltpu.VMEM((planes, GROUP, rows, chunk), bf16),
             pltpu.VMEM((half, GROUP, rows, chunk), bf16),
-            pltpu.VMEM((half, GROUP - 1, rows, chunk), bf16),
-            pltpu.VMEM((tile + 8, 256), jnp.float32),
+            pltpu.VMEM((half, 2, rows, chunk), bf16),
+            pltpu.VMEM((half, 2, rows // 2, chunk), bf16),
+            pltpu.VMEM((tile + 8, 256), f32),
             pltpu.VMEM((16, 2 * units), bf16),
             pltpu.VMEM((16, 2 * units), bf16),
-            dma((3,)),
-            dma((2, GROUP)),
+            pltpu.VMEM((8, 2 * units), f32),
+            pltpu.VMEM((GROUP, piece, 2 * units), bf16),
+            pltpu.VMEM((GROUP, units, out_piece), bf16),
+            pltpu.VMEM((rows, width), bf16),
+            pltpu.VMEM((piece, local), f32),
+            pltpu.VMEM((piece, local), f32),
+            pltpu.VMEM((local, out_piece), f32),
+            dma((6,)),
+            dma((3, GROUP)),
             dma((count,)),
             dma((count,)),
             dma((2, count)),
@@ -500,16 +646,33 @@
             dma((GROUP,)),
             dma((GROUP,)),
             dma((GROUP,)),
-            dma((2,)),
+            dma((4,)),
             dma((half, GROUP)),
             dma((half, GROUP)),
-            dma((half, GROUP)),
-            dma((half, GROUP)),
+            dma((half, 4)),
+            dma((half, 4)),
+            dma((half, 2)),
+            dma((half, 2)),
+            dma((count,)),
+            dma((2, count)),
         ],
         compiler_params=pltpu.CompilerParams(
             collective_id=0, has_side_effects=True, vmem_limit_bytes=67043328
         ),
-    )(normed, wu, wd, par, down_scale[None, :])
+    )(
+        tokens,
+        gate_weight,
+        value_weight,
+        down_weight,
+        norm_gain[None, :],
+        gate_scale[None, :],
+        value_scale[None, :],
+        gate_kernel,
+        value_kernel,
+        gate_bias[None, :],
+        value_bias[None, :],
+        down_scale[None, :],
+    )
 
 
 def solution(mesh):

time: 237 us -> 219 us (0.924); the launches traced: 235 us -> 219 us
  other arithmetic: 9.27 us -> 0 us
  local copies, waits for them, and re-layouts: 12.2 us -> 7.91 us
    broadcast_in_dim x4, local copies, waits for them, and re-layouts: 0.04 us -> 5.24 us  [the longest x1 1.31 us: grouped_body(): gate_scale[None, :]]
    convert_element_type x2 -> x0, other arithmetic: 4.65 us -> none  [the longest x1 2.42 us: normalize(): return (scaled * norm_gain[None, :]).astype(jnp.bfloat16)]
    transpose x1 -> x0, local copies, waits for them, and re-layouts: 4.48 us -> none  [grouped_body(): both = both.reshape(2, piece, GROUP, blocks, 128).transpose(2, 1, 3, 0, 4)]
    reshape x1 -> x0, local copies, waits for them, and re-layouts: 4.24 us -> none  [grouped_body(): wu = both.reshape(GROUP, piece, 2 * units)]
    reduce_sum x1 -> x0, other arithmetic: 2.72 us -> none  [normalize(): jnp.mean(values * values, axis=1, keepdims=True) + epsilon]
where the time goes in v2:
time: 219 us
  Pallas kernels  211 us (96%)
  local copies, waits for them, and re-layouts  7.91 us (4%)
    pallas_call x1, Pallas kernels, grouped_body(): pl.pallas_call(functools.partial(fused_kernel, planes), out_shape=jax.Sha...  211 us

profile of v2, /device:TPU:1, one launch (start us, length us, event | category | flops | bytes accessed | tf_op | source)
XLA Modules:
  0.0 219.0 jit_solution(1808214016390015542)
XLA Ops:
  0.0 1.3 broadcast_in_dim.19.gate_scale
  1.3 1.3 broadcast_in_dim.20.value_scale
  2.6 1.3 broadcast_in_dim.21.gate_bias
  3.9 1.3 broadcast_in_dim.22.value_bias
  5.2 211.1 %shard_map.118 = bf16[768,1024]{1,0:T(8,128)(2,1)} custom-call(bf16[768,2048]{1,0:T(8,128)(2,1)} %tok_hbm.1, f32[128,2560]{1,0:T(8,128)} %gate_hbm.1, f32[128,2560]{1,0:T(8,128)} %value_hbm.1, f32[2560,128]{1,0:T(8,128)} %down_hbm.1, f32[1,2048]{1,0:T(1,128)} %bitcast.2, f32[1,2560]{1,0:T(1,128)} %broadcast_in_dim.19.gate_scale, ...), custom_call_target="tpu_custom_call" | custom-call | tf_op jit(solution)/shard_map/pallas_call | solution.py:615
  216.3 2.7 %copy.14 = bf16[768,1024]{1,0:T(8,128)(2,1)} copy(bf16[768,1024]{1,0:T(8,128)(2,1)} %shard_map.118) | data formatting | bytes 3145728

commit v3 on v2

--- a/solution.py
+++ b/solution.py
@@ -408,6 +408,7 @@
 
     tiles = all_rows // tile
     slots = (2 * planes - 2) * GROUP
+    per_tile = -(-slots // (early // 256 * tiles))
 
     def late_slot(slot):
         q, below = plane_of(slot // GROUP + 1)
@@ -430,11 +431,12 @@
             act = 0.5 * g * (1.0 + jnp.tanh(math.sqrt(2.0 / math.pi) * (g + 0.044715 * (g * g * g))))
             hidden[rows, pl.ds(pl.multiple_of(j * 128, 128), 128)] = (act * v).astype(jnp.bfloat16)
             taps[0:8, :] = taps[tile : tile + 8, :]
-            slot = j * tiles + m
-
-            @pl.when((slot < slots) & (j < early // 256))
-            def _():
-                late_slot(slot)
+            for k in range(per_tile):
+                slot = (j * tiles + m) * per_tile + k
+
+                @pl.when((slot < slots) & (j < early // 256))
+                def _():
+                    late_slot(slot)
 
             return inner
 
@@ -444,12 +446,6 @@
     halo_part(0, 0, early_blocks)
     lax.fori_loop(0, early_blocks, column_step, 0)
 
-    def late_rest(slot, carry):
-        late_slot(slot)
-        return carry
-
-    if early_blocks * tiles < slots:
-        lax.fori_loop(early_blocks * tiles, slots, late_rest, 0)
     for direction in (0, 1):
         forward(1, direction, me)
     own_plane(1)
@@ -607,7 +603,7 @@
     out_piece = down_weight.shape[1]
     units = local // GROUP
     chunk = GROUP * out_piece
-    tile = rows // 2
+    tile = rows
     dma = pltpu.SemaphoreType.DMA
     bf16, f32 = jnp.bfloat16, jnp.float32
     vmem = pl.BlockSpec(memory_space=pltpu.VMEM)

time: 219 us -> 218 us (level)
  no operation moved by 1% of the time
where the time goes in v3:
time: 218 us
  Pallas kernels  210 us (96%)
  local copies, waits for them, and re-layouts  7.91 us (4%)
    pallas_call x1, Pallas kernels, grouped_body(): pl.pallas_call(functools.partial(fused_kernel, planes), out_shape=jax.Sha...  210 us

profile of v3, /device:TPU:1, one launch (start us, length us, event | category | flops | bytes accessed | tf_op | source)
XLA Modules:
  0.0 218.0 jit_solution(5143176059963249508)
XLA Ops:
  0.0 1.3 broadcast_in_dim.19.gate_scale
  1.3 1.3 broadcast_in_dim.20.value_scale
  2.6 1.3 broadcast_in_dim.21.gate_bias
  3.9 1.3 broadcast_in_dim.22.value_bias
  5.2 210.1 %shard_map.118 = bf16[768,1024]{1,0:T(8,128)(2,1)} custom-call(bf16[768,2048]{1,0:T(8,128)(2,1)} %tok_hbm.1, f32[128,2560]{1,0:T(8,128)} %gate_hbm.1, f32[128,2560]{1,0:T(8,128)} %value_hbm.1, f32[2560,128]{1,0:T(8,128)} %down_hbm.1, f32[1,2048]{1,0:T(1,128)} %bitcast.2, f32[1,2560]{1,0:T(1,128)} %broadcast_in_dim.19.gate_scale, ...), custom_call_target="tpu_custom_call" | custom-call | tf_op jit(solution)/shard_map/pallas_call | solution.py:611
  215.3 2.7 %copy.14 = bf16[768,1024]{1,0:T(8,128)(2,1)} copy(bf16[768,1024]{1,0:T(8,128)(2,1)} %shard_map.118) | data formatting | bytes 3145728
